TPU v7x, 32 devices: a whole 2x2x4 slice. The times are simulated.
32 devices in a mesh: fs: 8 (over z, y), tp: 4 (over x, core).
Axes of the slice: x: 2, y: 2, z: 4, core: 2. Of those that a mesh axis runs over, the one named last changes fastest.
Arguments:
- stream: bfloat16 [3072, 2048], P('fs', 'tp'), may hold values from -3 to 3
- gain_first: float32 [2048], replicated, may hold values from 0.1 to 1.9
- gain_mixer: float32 [2048], replicated, may hold values from 0.1 to 1.9
- gain_second: float32 [2048], replicated, may hold values from 0.1 to 1.9
- gate_weight: float32 [2048, 5632], P('fs', 'tp'), may hold values from -0.125 to 0.125
- gate_scale: float32 [5632], P('tp'), may hold values from 0.5 to 2
- up_weight: float32 [2048, 5632], P('fs', 'tp'), may hold values from -0.125 to 0.125
- up_scale: float32 [5632], P('tp'), may hold values from 0.5 to 2
- down_weight: float32 [5632, 2048], P('tp', 'fs'), may hold values from -0.109375 to 0.109375
- down_scale: float32 [2048], P('tp'), may hold values from 0.5 to 2
- pool_in_weight: float32 [2048, 512], P('fs', 'tp'), may hold values from -0.125 to 0.125
- pool_in_scale: float32 [512], P('tp'), may hold values from 0.5 to 2
- pool_out_weight: float32 [512, 2048], P('tp', 'fs'), may hold values from -0.375 to 0.375
- pool_out_scale: float32 [2048], P('tp'), may hold values from 0.5 to 2
Outputs:
- layer_out: bfloat16 [3072, 2048], P('fs', 'tp')
All inputs are finite; a program needn't handle non-finite values.
Results may differ from a plain program's by a relative error of at most 0.025.
Values may be sent and summed in bfloat16 or wider, within the bound.
A program may use at most 64 MiB of HBM per device.

v0:
```python
import jax
import jax.numpy as jnp
from jax import lax
from jax.sharding import PartitionSpec as P

SEQ = 128


eps = 1e-06
WINDOWS = (2, 4, 8, 16)


def normed(own_columns, norm_gain):
    gathered = lax.all_gather(own_columns, "tp", axis=1, tiled=True)
    floats = gathered.astype(jnp.float32)
    scaled = floats * lax.rsqrt(jnp.mean(floats * floats, axis=-1, keepdims=True) + eps)
    return (scaled * norm_gain).astype(jnp.bfloat16)


def residual_add(own_columns, partial_value, column_scale, factor):
    summed = lax.psum_scatter(
        partial_value.astype(jnp.bfloat16), "tp", scatter_dimension=1, tiled=True
    ).astype(jnp.float32)
    return (own_columns.astype(jnp.float32) + factor * (summed * column_scale)).astype(jnp.bfloat16)


def pooling(pool_input):
    channels = pool_input.shape[1]
    floats = pool_input.astype(jnp.float32).reshape(-1, SEQ, channels)
    csum = jnp.concatenate(
        [jnp.zeros((floats.shape[0], 1, channels), jnp.float32), jnp.cumsum(floats, axis=1)], axis=1
    )
    position = jnp.arange(SEQ)
    channel_index = lax.axis_index("tp") * channels + jnp.arange(channels, dtype=jnp.int32)
    channel_group = channel_index * 4 // (channels * lax.axis_size("tp"))
    pooled = -floats
    for group_index, window in enumerate(WINDOWS):
        before = window // 2
        after_span = window - before
        upper_sum = jnp.pad(csum, ((0, 0), (0, after_span), (0, 0)), mode="edge")[
            :, after_span : after_span + SEQ
        ]
        lower_sum = jnp.pad(csum, ((0, 0), (before, 0), (0, 0)), mode="edge")[:, :SEQ]
        counts = (
            jnp.minimum(position + after_span, SEQ) - jnp.maximum(position - before, 0)
        ).astype(jnp.float32)
        window_mean = (upper_sum - lower_sum) / counts[None, :, None]
        select = (channel_group == group_index).astype(jnp.float32)
        pooled = pooled + window_mean * select
    return pooled.reshape(-1, channels).astype(jnp.bfloat16)


def body(
    stream,
    gain_first,
    gain_mixer,
    gain_second,
    gate_weight,
    gate_scale,
    up_weight,
    up_scale,
    down_weight,
    down_scale,
    pool_in_weight,
    pool_in_scale,
    pool_out_weight,
    pool_out_scale,
):
    gate_half = gate_weight.astype(jnp.bfloat16)
    up_half = up_weight.astype(jnp.bfloat16)
    down_half = down_weight.astype(jnp.bfloat16)
    in_half = pool_in_weight.astype(jnp.bfloat16)
    out_half = pool_out_weight.astype(jnp.bfloat16)
    in_whole, out_whole = (
        lax.all_gather(in_half, "fs", axis=0, tiled=True),
        lax.all_gather(out_half, "fs", axis=1, tiled=True),
    )
    gate_whole, up_whole, down_whole = (
        lax.all_gather(gate_half, "fs", axis=0, tiled=True),
        lax.all_gather(up_half, "fs", axis=0, tiled=True),
        lax.all_gather(down_half, "fs", axis=1, tiled=True),
    )

    def feed_forward(normed_rows):
        gate_sum = jnp.dot(normed_rows, gate_whole, preferred_element_type=jnp.float32) * gate_scale
        up_sum = jnp.dot(normed_rows, up_whole, preferred_element_type=jnp.float32) * up_scale
        hidden = (jax.nn.silu(gate_sum) * up_sum).astype(jnp.bfloat16)
        return jnp.dot(hidden, down_whole, preferred_element_type=jnp.float32)

    after_first = residual_add(stream, feed_forward(normed(stream, gain_first)), down_scale, 0.5)
    mixer_normed = normed(after_first, gain_mixer)
    pool_input = (
        jnp.dot(mixer_normed, in_whole, preferred_element_type=jnp.float32) * pool_in_scale
    ).astype(jnp.bfloat16)
    pooled = pooling(pool_input)
    tp_count = lax.axis_size("tp")
    all_pooled = lax.all_gather(pooled, "tp", axis=1, tiled=True)
    out_columns = lax.all_to_all(out_whole, "tp", split_axis=1, concat_axis=0, tiled=True)
    block_width = out_columns.shape[0] // tp_count
    pooled_blocks = all_pooled.reshape(all_pooled.shape[0], tp_count, block_width)
    weight_blocks = out_columns.reshape(tp_count, block_width, out_columns.shape[1])
    partials = jnp.einsum(
        "rbc,bcd->brd", pooled_blocks, weight_blocks, preferred_element_type=jnp.float32
    ).astype(jnp.bfloat16)
    mixed = jnp.sum(partials.astype(jnp.float32), axis=0)
    after_mix = (after_first.astype(jnp.float32) + mixed * pool_out_scale).astype(jnp.bfloat16)
    return residual_add(after_mix, feed_forward(normed(after_mix, gain_second)), down_scale, 0.5)


def solution(mesh):
    placed = (
        P("fs", "tp"),
        P(),
        P(),
        P(),
        P("fs", "tp"),
        P("tp"),
        P("fs", "tp"),
        P("tp"),
        P("tp", "fs"),
        P("tp"),
        P("fs", "tp"),
        P("tp"),
        P("tp", "fs"),
        P("tp"),
    )
    return jax.shard_map(body, mesh=mesh, in_specs=placed, out_specs=P("fs", "tp"), check_vma=False)
```

profile of v0, /device:TPU:0, one launch (start us, length us, event | category | flops | bytes accessed | tf_op | source)
XLA Modules:
  0.0 509.7 jit_solution(2998391872795220859)
XLA Ops:
  6.5 0.7 all-gather.7.cloned.1.call-update
  7.3 0.0 all-gather.9.cloned.1.call-start
  7.3 2.3 convert_element_type.144
  9.6 0.0 all-gather.9.cloned.1.call-update
  9.6 0.0 all-gather.11.cloned.1.call-start
  9.7 1.0 convert_element_type.145
  10.7 0.0 all-gather.11.cloned.1.call-update
  10.7 0.0 copy-start.11
  10.7 0.0 all-gather.13.cloned.1.call-start
  10.8 0.5 copy-done.6
  11.2 1.0 convert_element_type.147
  12.2 0.0 all-gather.13.cloned.1.call-update
  12.2 0.0 reduce-scatter.3.cloned.1.call-start
  12.3 19.0 %all-gather.7.cloned.1.call-done = bf16[384,2048]{1,0:T(8,128)(2,1)} async-done(((bf16[384,512]{1,0:T(8,128)(2,1)}), bf16[384,2048]{1,0:T(8,128)(2,1)}) %all-gather.7.cloned.1.call-update) | async-done | bytes 1572880 | tf_op jit(solution)/shard_map/all_gather | solution.py:14
  31.3 1.8 fusion
  33.1 92.7 %all-gather.9.cloned.1.call-done = bf16[2048,1408]{1,0:T(8,128)(2,1)} async-done(((bf16[256,1408]{1,0:T(8,128)(2,1)}), bf16[2048,1408]{1,0:T(8,128)(2,1)}) %all-gather.9.cloned.1.call-update) | async-done | bytes 5767184 | tf_op jit(solution)/shard_map/all_gather | solution.py:79
  125.8 7.1 %convolution_multiply_fusion.3 = f32[384,1408]{1,0:T(8,128)} fusion(bf16[2048,1408]{1,0:T(8,128)(2,1)} %all-gather.9.cloned.1.call-done, f32[1408]{0:T(1024)S(1)} %copy-done.13, bf16[384,2048]{1,0:T(8,128)(2,1)} %all-gather.7.cloned.1.call-done, f32[2048]{0:T(1024)S(1)} %copy-done.11, f32[384]{0:T(512)S(1)} %add_rsqrt_fusion.2), kind=kOutput, calls=%fused_computation.21 | convolution fusion | flops 2218278912 | bytes 9518080 | tf_op jit(solution)/shard_map/dot_general | solution.py:85
  133.0 85.6 %all-gather.11.cloned.1.call-done = bf16[2048,1408]{1,0:T(8,128)(2,1)} async-done(((bf16[256,1408]{1,0:T(8,128)(2,1)}), bf16[2048,1408]{1,0:T(8,128)(2,1)}) %all-gather.11.cloned.1.call-update) | async-done | bytes 5767184 | tf_op jit(solution)/shard_map/all_gather | solution.py:80
  218.5 93.2 %all-gather.13.cloned.1.call-done = bf16[1408,2048]{1,0:T(8,128)(2,1)} async-done(((bf16[1408,256]{1,0:T(8,128)(2,1)}), bf16[1408,2048]{1,0:T(8,128)(2,1)}) %all-gather.13.cloned.1.call-update) | async-done | bytes 5767184 | tf_op jit(solution)/shard_map/all_gather | solution.py:81
  311.8 11.2 %convolution_convert_fusion.1 = bf16[384,2048]{1,0:T(8,128)(2,1)} fusion(bf16[1408,2048]{1,0:T(8,128)(2,1)} %all-gather.13.cloned.1.call-done, bf16[2048,1408]{1,0:T(8,128)(2,1)} %all-gather.11.cloned.1.call-done, f32[384,1408]{1,0:T(8,128)} %convolution_multiply_fusion.3, f32[1408]{0:T(1024)S(1)} %copy-done.14, bf16[384,2048]{1,0:T(8,128)(2,1)S(1)} %copy-done.2, ...), kind=kOutput, calls=%fused_computation.23 | convolution fusion | flops 4436901888 | bytes 16858112 | tf_op jit(solution)/shard_map/dot_general | solution.py:88
  323.0 0.0 reduce-scatter.3.cloned.1.call-update
  323.0 0.0 all-gather.15.cloned.1.call-start
  323.1 26.3 %reduce-scatter.3.cloned.1.call-done = bf16[384,512]{1,0:T(8,128)(2,1)} async-done(((bf16[384,2048]{1,0:T(8,128)(2,1)}), bf16[384,512]{1,0:T(8,128)(2,1)}) %reduce-scatter.3.cloned.1.call-update) | async-done | bytes 393232 | tf_op jit(solution)/shard_map/reduce_scatter | solution.py:21
  349.3 1.9 add_convert_fusion.2
  351.2 0.0 all-gather.15.cloned.1.call-update
  351.3 0.1 copy.16
  351.4 31.7 %all_gather.34 = bf16[128,2048]{0,1:T(8,128)(2,1)S(1)} all-gather(bf16[128,256]{0,1:T(8,128)(2,1)S(1)} %copy.16), channel_id=1, replica_groups=mesh['fs'=8,'tp'=4] {'fs'}, dimensions={1}, use_global_device_ids=true | all-gather | bytes 589824 | tf_op jit(solution)/shard_map/all_gather | solution.py:76
  383.1 1.0 copy.17
  384.1 3.5 all-to-all-start
  387.6 0.0 all-gather.17.cloned.1.call-start
  387.8 31.5 %all_gather.32 = bf16[2048,128]{1,0:T(8,128)(2,1)S(1)} all-gather(bf16[256,128]{1,0:T(8,128)(2,1)S(1)} %convert_element_type.154), channel_id=1, replica_groups=mesh['fs'=8,'tp'=4] {'fs'}, dimensions={0}, use_global_device_ids=true | all-gather | bytes 589824 | tf_op jit(solution)/shard_map/all_gather | solution.py:75
  419.3 1.8 fusion.3
  421.1 2.0 fusion.20
  423.2 0.2 reduce_window_sum.11
  423.5 0.3 fusion.46
  423.8 0.1 copy.15
  423.9 6.7 %all_gather.33 = bf16[384,512]{0,1:T(8,128)(2,1)S(1)} all-gather(bf16[384,128]{0,1:T(8,128)(2,1)S(1)} %copy.15), channel_id=1, replica_groups=mesh['fs'=8,'tp'=4] {'tp'}, dimensions={1}, use_global_device_ids=true | all-gather | bytes 491520 | tf_op jit(solution)/shard_map/all_gather | solution.py:97
  430.6 0.6 convert_reduce_fusion
  431.2 0.9 add_convert_fusion.1
  432.1 0.0 all-gather.17.cloned.1.call-update
  432.1 0.2 reduce-scatter.5.cloned.1.call-start
  432.4 20.1 %all-gather.17.cloned.1.call-done = bf16[384,2048]{1,0:T(8,128)(2,1)} async-done(((bf16[384,512]{1,0:T(8,128)(2,1)}), bf16[384,2048]{1,0:T(8,128)(2,1)}) %all-gather.17.cloned.1.call-update) | async-done | bytes 1572880 | tf_op jit(solution)/shard_map/all_gather | solution.py:14
  452.4 1.8 fusion.6
  454.3 7.2 %convolution_multiply_fusion.1 = f32[384,1408]{1,0:T(8,128)} fusion(bf16[2048,1408]{1,0:T(8,128)(2,1)} %all-gather.9.cloned.1.call-done, f32[1408]{0:T(1024)S(1)} %copy-done.13, bf16[384,2048]{1,0:T(8,128)(2,1)} %all-gather.17.cloned.1.call-done, f32[2048]{0:T(1024)S(1)} %copy-done.15, f32[384]{0:T(512)S(1)} %add_rsqrt_fusion), kind=kOutput, calls=%fused_computation.18 | convolution fusion | flops 2218278912 | bytes 9518080 | tf_op jit(solution)/shard_map/dot_general | solution.py:85
  461.5 11.3 %convolution_convert_fusion = bf16[384,2048]{1,0:T(8,128)(2,1)} fusion(bf16[1408,2048]{1,0:T(8,128)(2,1)} %all-gather.13.cloned.1.call-done, bf16[2048,1408]{1,0:T(8,128)(2,1)} %all-gather.11.cloned.1.call-done, f32[384,1408]{1,0:T(8,128)} %convolution_multiply_fusion.1, f32[1408]{0:T(1024)S(1)} %copy-done.14, bf16[384,2048]{1,0:T(8,128)(2,1)S(1)} %copy-done.3, ...), kind=kOutput, calls=%fused_computation.22 | convolution fusion | flops 4436901888 | bytes 16858112 | tf_op jit(solution)/shard_map/dot_general | solution.py:88
  472.8 0.0 reduce-scatter.5.cloned.1.call-update
  472.8 28.1 %reduce-scatter.5.cloned.1.call-done = bf16[384,512]{1,0:T(8,128)(2,1)} async-done(((bf16[384,2048]{1,0:T(8,128)(2,1)}), bf16[384,512]{1,0:T(8,128)(2,1)}) %reduce-scatter.5.cloned.1.call-update) | async-done | bytes 393232 | tf_op jit(solution)/shard_map/reduce_scatter | solution.py:21
  501.0 1.9 add_convert_fusion
  (54 shorter events, 0.2 us)
Async XLA Ops:
  6.5 3.2 copy-start.5
  6.5 24.7 %all-gather.7.cloned.1.call-start = ((), (), s32[]{:S(2)}) async-start(), calls=%async_computation.3 | async-start | bytes 1966080 | tf_op jit(solution)/shard_map/all_gather | solution.py:14
  7.3 118.5 %all-gather.9.cloned.1.call-start = ((), (), s32[]{:S(2)}) async-start(), calls=%async_computation.4 | async-start | bytes 6488064 | tf_op jit(solution)/shard_map/all_gather | solution.py:79
  9.6 1.6 copy-start.6
  9.6 208.9 %all-gather.11.cloned.1.call-start = ((), (), s32[]{:S(2)}) async-start(), calls=%async_computation.5 | async-start | bytes 6488064 | tf_op jit(solution)/shard_map/all_gather | solution.py:80
  10.7 115.1 %copy-start.11 = (f32[2048]{0:T(1024)S(1)}, f32[2048]{0:T(1024)}, u32[]{:S(2)}) copy-start(f32[2048]{0:T(1024)} %param.15) | copy-start | bytes 24580
  10.7 115.1 %copy-start.13 = (f32[1408]{0:T(1024)S(1)}, f32[1408]{0:T(1024)}, u32[]{:S(2)}) copy-start(f32[1408]{0:T(1024)} %param.19) | copy-start | bytes 16900
  10.7 301.1 %all-gather.13.cloned.1.call-start = ((), (), s32[]{:S(2)}) async-start(), calls=%async_computation.6 | async-start | bytes 6488064 | tf_op jit(solution)/shard_map/all_gather | solution.py:81
  12.2 337.1 %reduce-scatter.3.cloned.1.call-start = ((), (), s32[]{:S(2)}) async-start(), calls=%async_computation.7 | async-start | bytes 1966080 | tf_op jit(solution)/shard_map/reduce_scatter | solution.py:21
  33.1 278.7 %copy-start.2 = (bf16[384,2048]{1,0:T(8,128)(2,1)S(1)}, bf16[384,2048]{1,0:T(8,128)(2,1)}, u32[]{:S(2)}) copy-start(bf16[384,2048]{1,0:T(8,128)(2,1)} %all-gather.7.cloned.1.call-done) | copy-start | bytes 4718596
  33.1 278.7 %copy-start.14 = (f32[1408]{0:T(1024)S(1)}, f32[1408]{0:T(1024)}, u32[]{:S(2)}) copy-start(f32[1408]{0:T(1024)} %param.21) | copy-start | bytes 16900
  133.0 216.4 %copy-start.4 = (bf16[384,512]{1,0:T(8,128)(2,1)S(1)}, bf16[384,512]{1,0:T(8,128)(2,1)}, u32[]{:S(2)}) copy-start(bf16[384,512]{1,0:T(8,128)(2,1)} %param.14) | copy-start | bytes 1179652
  133.0 216.4 %copy-start.9 = (f32[512]{0:T(512)S(1)}, f32[512]{0:T(512)}, u32[]{:S(2)}) copy-start(f32[512]{0:T(512)} %param.23) | copy-start | bytes 6148
  323.0 28.3 %copy-start.7 = (f32[128,256]{1,0:T(8,128)S(1)}, f32[128,256]{1,0:T(8,128)}, u32[]{:S(2)}) copy-start(f32[128,256]{1,0:T(8,128)} %param.26) | copy-start | bytes 393220
  323.0 64.6 %copy-start.8 = (f32[256,128]{1,0:T(8,128)S(1)}, f32[256,128]{1,0:T(8,128)}, u32[]{:S(2)}) copy-start(f32[256,128]{1,0:T(8,128)} %param.24) | copy-start | bytes 393220
  323.0 96.3 %all-gather.15.cloned.1.call-start = ((), (), s32[]{:S(2)}) async-start(), calls=%async_computation.8 | async-start | bytes 1966080 | tf_op jit(solution)/shard_map/all_gather | solution.py:14
  383.1 38.0 %copy-start.12 = (f32[2048]{0:T(1024)S(1)}, f32[2048]{0:T(1024)}, u32[]{:S(2)}) copy-start(f32[2048]{0:T(1024)} %param.16) | copy-start | bytes 24580
  383.1 38.0 %copy-start.16 = (f32[128]{0:T(128)S(1)}, f32[128]{0:T(128)}, u32[]{:S(2)}) copy-start(f32[128]{0:T(128)} %param.25) | copy-start | bytes 1540
  384.1 46.5 %all-to-all-start = ((bf16[128,4,512]{2,0,1:T(8,128)(2,1)}), bf16[128,4,512]{2,0,1:T(8,128)(2,1)S(1)}, u32[]{:S(2)}, u32[]{:S(2)}) async-start(bf16[128,4,512]{2,0,1:T(8,128)(2,1)} %copy.17), calls=%async_computation.1 | async-start | bytes 1048576 | tf_op jit(solution)/shard_map/all_to_all | solution.py:98
  387.6 64.9 %all-gather.17.cloned.1.call-start = ((), (), s32[]{:S(2)}) async-start(), calls=%async_computation.9 | async-start | bytes 1966080 | tf_op jit(solution)/shard_map/all_gather | solution.py:14
  423.2 8.0 %copy-start = (bf16[384,512]{1,0:T(8,128)(2,1)S(1)}, bf16[384,512]{1,0:T(8,128)(2,1)}, u32[]{:S(2)}) copy-start(bf16[384,512]{1,0:T(8,128)(2,1)} %add_convert_fusion.2) | copy-start | bytes 1179652
  423.2 8.0 %copy-start.10 = (f32[512]{0:T(512)S(1)}, f32[512]{0:T(512)}, u32[]{:S(2)}) copy-start(f32[512]{0:T(512)} %param.27) | copy-start | bytes 6148
  431.2 23.0 %copy-start.15 = (f32[2048]{0:T(1024)S(1)}, f32[2048]{0:T(1024)}, u32[]{:S(2)}) copy-start(f32[2048]{0:T(1024)} %param.17) | copy-start | bytes 24580
  432.1 68.8 %reduce-scatter.5.cloned.1.call-start = ((), (), s32[]{:S(2)}) async-start(), calls=%async_computation.10 | async-start | bytes 1966080 | tf_op jit(solution)/shard_map/reduce_scatter | solution.py:21
  454.3 7.3 %copy-start.3 = (bf16[384,2048]{1,0:T(8,128)(2,1)S(1)}, bf16[384,2048]{1,0:T(8,128)(2,1)}, u32[]{:S(2)}) copy-start(bf16[384,2048]{1,0:T(8,128)(2,1)} %all-gather.17.cloned.1.call-done) | copy-start | bytes 4718596
  461.5 39.4 %copy-start.1 = (bf16[384,512]{1,0:T(8,128)(2,1)S(1)}, bf16[384,512]{1,0:T(8,128)(2,1)}, u32[]{:S(2)}) copy-start(bf16[384,512]{1,0:T(8,128)(2,1)} %add_convert_fusion.1) | copy-start | bytes 1179652
Sparse Core Ops, SparseCore 0:
  8.9 22.3 all-gather.6
  33.5 92.2 all-gather.8
  128.0 90.4 all-gather.10
  220.4 91.2 all-gather.12
  323.1 26.1 reduce-scatter.2
  351.4 19.6 all-gather.14
  432.3 20.1 all-gather.16
  472.9 27.9 reduce-scatter.4
where the time goes:
time: 510 us
  waiting for transfers between devices  366 us (72%)
  blocking collectives  69.9 us (14%)
  matrix products  39.5 us (8%)
  other arithmetic  14.9 us (3%)
  between operations  13.8 us (3%)
    all_gather x1, waiting for transfers between devices, body(): lax.all_gather(down_half, 'fs', axis=1, tiled=True)  93.2 us
    all_gather x1, waiting for transfers between devices, body(): lax.all_gather(gate_half, 'fs', axis=0, tiled=True)  92.7 us
    all_gather x1, waiting for transfers between devices, body(): lax.all_gather(up_half, 'fs', axis=0, tiled=True)  85.6 us
    reduce_scatter x2, waiting for transfers between devices, residual_add(): lax.psum_scatter(partial_value.astype(jnp.bfloat16), 'tp', scatter_dimens...  54.4 us
    all_gather x3, waiting for transfers between devices, normed(): gathered = lax.all_gather(own_columns, 'tp', axis=1, tiled=True)  39.1 us
    all_gather x1, blocking collectives, body(): lax.all_gather(out_half, 'fs', axis=1, tiled=True)  31.7 us
    all_gather x1, blocking collectives, body(): lax.all_gather(in_half, 'fs', axis=0, tiled=True)  31.5 us
    dot_general x2, matrix products, feed_forward(): return jnp.dot(hidden, down_whole, preferred_element_type=jnp.float32)  22.5 us
  transfers between devices with their start and end apart: 9, of which 7 were waited for; matrix products, arithmetic and copies ran while one was open for 4% of the time, Pallas kernels for 0%

commit v1 on v0

v1 whole, which is shorter than its diff:
```python
import functools

import jax
import jax.numpy as jnp
from jax import lax
from jax.experimental import pallas as pl
from jax.experimental.pallas import tpu as pltpu
from jax.sharding import PartitionSpec as P

SEQ = 128
MESH = pl.DeviceIdType.MESH

eps = 1e-06
WINDOWS = (2, 4, 8, 16)


def fs_grid(count):
    ny = 1
    while (2 * ny) * (2 * ny) <= count and count % (2 * ny) == 0:
        ny *= 2
    return ny, count // ny


def gather_kernel(nfs, ntp, pool, gate, up, down, stream, pool_all, gate_all, up_all, down_all, stream_all,
                  send_sem, recv_sem, local_sem, tsend, trecv, psend, precv):
    ny, nz = fs_grid(nfs)
    nx = ntp // 2
    fs, tp = lax.axis_index("fs"), lax.axis_index("tp")
    z, y = fs // ny, fs % ny
    x, core = tp // 2, tp % 2
    partner = x * 2 + (1 - core)
    alternate = ny == 2 and nz > 1

    barrier = pltpu.get_barrier_semaphore()

    def greet(cond, f, t):
        @pl.when(cond)
        def _():
            pl.semaphore_signal(barrier, inc=1, device_id={"fs": f, "tp": t}, device_id_type=MESH)

    greet(z > 0, fs - ny, tp)
    greet(z < nz - 1, fs + ny, tp)
    greet(y > 0, fs - 1, tp)
    greet(y < ny - 1, fs + 1, tp)
    pl.semaphore_signal(barrier, inc=1, device_id={"fs": fs, "tp": partner}, device_id_type=MESH)
    for k in range(1, nx):
        pl.semaphore_signal(
            barrier, inc=1, device_id={"fs": fs, "tp": (x + k) % nx * 2 + core}, device_id_type=MESH
        )
    peers = nx
    for cond in (z > 0, z < nz - 1, y > 0, y < ny - 1):
        peers = peers + jnp.where(cond, 1, 0)
    pl.semaphore_wait(barrier, peers)

    pieces = [(lambda: pool, lambda f: pool_all.at[tp, f])]
    for own, whole in ((gate, gate_all), (up, up_all), (down, down_all)):
        rows = own.shape[0]
        halves = 2 if alternate else 1
        for h in range(halves):
            part = pl.ds(h * (rows // halves), rows // halves)
            pieces.append((
                functools.partial(lambda own, part: own.at[part], own, part),
                functools.partial(lambda whole, part, f: whole.at[f, part], whole, part),
            ))
    started = []

    def remote(piece, f, direction, target, mine=False):
        own, whole = pieces[piece]
        return pltpu.make_async_remote_copy(
            src_ref=own() if mine else whole(f),
            dst_ref=whole(f),
            send_sem=send_sem.at[piece, f, direction],
            recv_sem=recv_sem.at[piece, f],
            device_id={"fs": target, "tp": tp},
            device_id_type=MESH,
        )

    def send(cond, piece, f, direction, mine=False):
        target = fs + (-ny, ny, -1, 1)[direction]

        @pl.when(cond)
        def _():
            remote(piece, f, direction, target, mine).start()

        started.append((cond, piece, f, direction, target, mine))

    def arrived(cond, piece, f):
        @pl.when(cond)
        def _():
            remote(piece, f, 0, fs, False).wait_recv()

    def by_y(cond, piece, f, mine=False):
        send(cond & (y > 0), piece, f, 2, mine)
        send(cond & (y < ny - 1), piece, f, 3, mine)

    yes = z >= 0

    def stream_copy(src, slot, t_target, k):
        return pltpu.make_async_remote_copy(
            src_ref=src, dst_ref=stream_all.at[slot], send_sem=tsend.at[k], recv_sem=trecv.at[slot],
            device_id={"fs": fs, "tp": t_target}, device_id_type=MESH)

    def pool_copy(slot, t_target, k):
        return pltpu.make_async_remote_copy(
            src_ref=pool_all.at[slot], dst_ref=pool_all.at[slot], send_sem=psend.at[k], recv_sem=precv.at[slot],
            device_id={"fs": fs, "tp": t_target}, device_id_type=MESH)

    npieces = len(pieces)
    locals_ = [pltpu.make_async_copy(own(), whole(fs), local_sem.at[i]) for i, (own, whole) in enumerate(pieces)]
    locals_.append(pltpu.make_async_copy(stream, stream_all.at[tp], local_sem.at[npieces]))
    for piece in range(npieces):
        send(z > 0, piece, fs, 0, True)
        send(z < nz - 1, piece, fs, 1, True)
        by_y(yes, piece, fs, True)
    stream_sends = []
    for k in range(1, nx):
        stream_sends.append(stream_copy(stream, tp, (x + k) % nx * 2 + core, k - 1))
    stream_sends.append(stream_copy(stream, tp, partner, nx - 1))
    for copy in stream_sends:
        copy.start()
    for copy in locals_:
        copy.start()

    def row_arrivals(piece, d, alt):
        low, high = fs - d * ny, fs + d * ny
        has_low, has_high = z >= d, z + d <= nz - 1
        for cond, f, direction, ahead, end in (
            (has_low, low, 1, z < nz - 1, z == d),
            (has_high, high, 0, z > 0, z + d == nz - 1),
        ):
            arrived(cond, piece, f)
            send(cond & ahead, piece, f, direction)
            if alt:
                by_y(cond & jnp.logical_not(end), piece, f)
                other = f + 1 - 2 * y
                arrived(cond & end, piece, other)
                send(cond & end & ahead, piece, other, direction)
            else:
                by_y(cond, piece, f)

    def column_arrivals(piece, alt):
        for d in range(nz):
            for sign in ((1,) if d == 0 else (-1, 1)):
                row_ok = (z + sign * d >= 0) & (z + sign * d <= nz - 1)
                if alt:
                    at = z + sign * d
                    if d == 0:
                        continue
                    row_ok = row_ok & (at != 0) & (at != nz - 1)
                base = fs + sign * d * ny
                for e in range(1, ny):
                    for step, direction, ok, ahead in (
                        (-e, 3, y >= e, y < ny - 1),
                        (e, 2, y + e <= ny - 1, y > 0),
                    ):
                        arrived(row_ok & ok, piece, base + step)
                        if ny > 2:
                            send(row_ok & ok & ahead, piece, base + step, direction)

    is_alt = [alternate and p > 0 and p % 2 == 0 for p in range(npieces)]

    for d in range(1, nz):
        row_arrivals(0, d, False)
    column_arrivals(0, False)
    locals_[0].wait()
    pool_sends = [pool_copy(tp, (x + k) % nx * 2 + core, k - 1) for k in range(1, nx)]
    pool_sends.append(pool_copy(tp, partner, nx - 1))
    for copy in pool_sends:
        copy.start()
    for k in range(1, nx):
        slot = (x + k) % nx * 2 + core
        stream_copy(stream, slot, partner, 0).wait_recv()
        copy = stream_copy(stream_all.at[slot], slot, partner, nx - 1 + k)
        copy.start()
        stream_sends.append(copy)

    for p in range(npieces):
        if is_alt[p]:
            other = fs + 1 - 2 * y
            arrived(yes, p, other)
            send(z == 0, p, other, 1)
            send(z == nz - 1, p, other, 0)
    for d in range(1, nz):
        for p in range(1, npieces):
            row_arrivals(p, d, is_alt[p])
        if d == 1:
            for k in range(1, nx):
                slot = (x + k) % nx * 2 + core
                pool_copy(slot, partner, 0).wait_recv()
                copy = pool_copy(slot, partner, nx - 1 + k)
                copy.start()
                pool_sends.append(copy)
    for p in range(1, npieces):
        column_arrivals(p, is_alt[p])
    for k in range(nx):
        slot = (x + k) % nx * 2 + (1 - core)
        stream_copy(stream, slot, partner, 0).wait_recv()
        pool_copy(slot, partner, 0).wait_recv()
    for copy in locals_[1:]:
        copy.wait()
    for copy in stream_sends + pool_sends:
        copy.wait_send()
    for cond, piece, f, direction, target, mine in started:
        @pl.when(cond)
        def _():
            remote(piece, f, direction, target, mine).wait_send()


def gather_all(nfs, ntp, pool, gate, up, down, stream):
    ny, nz = fs_grid(nfs)
    nx = ntp // 2
    npieces = 7 if (ny == 2 and nz > 1) else 4
    dtype = jnp.bfloat16
    any_spec = pl.BlockSpec(memory_space=pl.ANY)
    return pl.pallas_call(
        functools.partial(gather_kernel, nfs, ntp),
        name="collect_weights",
        out_shape=(
            jax.ShapeDtypeStruct((ntp, nfs) + pool.shape, dtype),
            jax.ShapeDtypeStruct((nfs,) + gate.shape, dtype),
            jax.ShapeDtypeStruct((nfs,) + up.shape, dtype),
            jax.ShapeDtypeStruct((nfs,) + down.shape, dtype),
            jax.ShapeDtypeStruct((ntp,) + stream.shape, dtype),
        ),
        in_specs=[any_spec] * 5,
        out_specs=[any_spec] * 5,
        scratch_shapes=[
            pltpu.SemaphoreType.DMA((npieces, nfs, 4)),
            pltpu.SemaphoreType.DMA((npieces, nfs)),
            pltpu.SemaphoreType.DMA((npieces + 1,)),
            pltpu.SemaphoreType.DMA((2 * nx,)),
            pltpu.SemaphoreType.DMA((ntp,)),
            pltpu.SemaphoreType.DMA((2 * nx,)),
            pltpu.SemaphoreType.DMA((ntp,)),
        ],
        compiler_params=pltpu.CompilerParams(collective_id=0, has_side_effects=True, vmem_limit_bytes=1 << 20),
    )(pool, gate, up, down, stream)


def sum_kernel(ntp, gathers, pieces, partial, resid, scale, out, pair, pair_sum, cross, *sems):
    pair_send, pair_recv, cross_send, cross_recv = sems[:4]
    nx = ntp // 2
    tp, fs = lax.axis_index("tp"), lax.axis_index("fs")
    x, core = tp // 2, tp % 2
    partner = x * 2 + (1 - core)
    rows, width = resid.shape
    step = rows // pieces
    barrier = pltpu.get_barrier_semaphore()
    pl.semaphore_signal(barrier, inc=1, device_id={"fs": fs, "tp": partner}, device_id_type=MESH)
    for k in range(1, nx):
        pl.semaphore_signal(
            barrier, inc=1, device_id={"fs": fs, "tp": (x + k) % nx * 2 + core}, device_id_type=MESH
        )
    pl.semaphore_wait(barrier, nx)

    def remote(src, dst, send, recv, target):
        return pltpu.make_async_remote_copy(
            src_ref=src, dst_ref=dst, send_sem=send, recv_sem=recv,
            device_id={"fs": fs, "tp": target}, device_id_type=MESH)

    def columns(t):
        return pl.ds(pl.multiple_of(t * width, width), width)

    parts = [pl.ds(i * step, step) for i in range(pieces)]
    offsets = list(range(1, nx)) + [0]
    sends = []
    for k in offsets:
        for i, part in enumerate(parts):
            copy = remote(partial.at[part, columns((x + k) % nx * 2 + (1 - core))], pair.at[k, part],
                          pair_send.at[k, i], pair_recv.at[k, i], partner)
            copy.start()
            sends.append(copy)
    for k in offsets[:-1]:
        target = (x + k) % nx * 2 + core
        for i, part in enumerate(parts):
            remote(pair.at[k, part], pair.at[k, part], pair_send.at[k, i], pair_recv.at[k, i], partner).wait_recv()
            pair_sum[k - 1, part] = (
                partial[part, columns(target)].astype(jnp.float32) + pair[k, part].astype(jnp.float32)
            ).astype(jnp.bfloat16)
            copy = remote(pair_sum.at[k - 1, part], cross.at[k - 1, part],
                          cross_send.at[k - 1, i], cross_recv.at[k - 1, i], target)
            copy.start()
            sends.append(copy)
    factor = 0.5 * scale[...]
    for i, part in enumerate(parts):
        remote(pair.at[0, part], pair.at[0, part], pair_send.at[0, i], pair_recv.at[0, i], partner).wait_recv()
        total = partial[part, columns(tp)].astype(jnp.float32) + pair[0, part].astype(jnp.float32)
        for k in range(1, nx):
            remote(cross.at[k - 1, part], cross.at[k - 1, part], cross_send.at[k - 1, i],
                   cross_recv.at[k - 1, i], partner).wait_recv()
            total = total + cross[k - 1, part].astype(jnp.float32)
        result = (resid[part].astype(jnp.float32) + total * factor).astype(jnp.bfloat16)
        if not gathers:
            out[part] = result
            continue
        out[tp, part] = result
        gather_send, gather_recv = sems[4:]
        for k in range(1, nx):
            copy = remote(out.at[tp, part], out.at[tp, part], gather_send.at[k - 1, i], gather_recv.at[tp, i],
                          (x + k) % nx * 2 + core)
            copy.start()
            sends.append(copy)
        copy = remote(out.at[tp, part], out.at[tp, part], gather_send.at[nx - 1, i], gather_recv.at[tp, i], partner)
        copy.start()
        sends.append(copy)
    if gathers:
        for k in range(1, nx):
            slot = (x + k) % nx * 2 + core
            for i, part in enumerate(parts):
                remote(out.at[slot, part], out.at[slot, part], gather_send.at[0, i], gather_recv.at[slot, i],
                       partner).wait_recv()
                copy = remote(out.at[slot, part], out.at[slot, part], gather_send.at[nx - 1 + k, i],
                              gather_recv.at[slot, i], partner)
                copy.start()
                sends.append(copy)
        for k in range(nx):
            slot = (x + k) % nx * 2 + (1 - core)
            for i, part in enumerate(parts):
                remote(out.at[slot, part], out.at[slot, part], gather_send.at[0, i], gather_recv.at[slot, i],
                       partner).wait_recv()
    for copy in sends:
        copy.wait_send()


def summed(ntp, gathers, identity, partial, resid, scale):
    nx = ntp // 2
    rows, width = resid.shape
    pieces = 3 if rows % 48 == 0 else 1
    vmem = pl.BlockSpec(memory_space=pltpu.VMEM)
    dma = pltpu.SemaphoreType.DMA
    scratch = [
        pltpu.VMEM((nx, rows, width), jnp.bfloat16),
        pltpu.VMEM((max(nx - 1, 1), rows, width), jnp.bfloat16),
        pltpu.VMEM((max(nx - 1, 1), rows, width), jnp.bfloat16),
        dma((nx, pieces)), dma((nx, pieces)), dma((nx, pieces)), dma((nx, pieces)),
    ]
    if gathers:
        scratch += [dma((2 * nx, pieces)), dma((ntp, pieces))]
    return pl.pallas_call(
        functools.partial(sum_kernel, ntp, gathers, pieces),
        name="sum_and_share" if gathers else "sum_last",
        out_shape=jax.ShapeDtypeStruct(((ntp,) if gathers else ()) + (rows, width), jnp.bfloat16),
        in_specs=[vmem] * 3,
        out_specs=vmem,
        scratch_shapes=scratch,
        compiler_params=pltpu.CompilerParams(
            collective_id=identity, has_side_effects=True, vmem_limit_bytes=32 << 20
        ),
    )(partial, resid, scale.reshape(1, width))


def joined(blocks):
    return jnp.swapaxes(blocks, 0, 1).reshape(blocks.shape[1], -1)


def rms(floats, norm_gain):
    scaled = floats * lax.rsqrt(jnp.mean(floats * floats, axis=-1, keepdims=True) + eps)
    return (scaled * norm_gain).astype(jnp.bfloat16)


def window_weights():
    position = jnp.arange(SEQ)
    rows, cols = position[:, None], position[None, :]
    mats = []
    for window in WINDOWS:
        low = jnp.maximum(rows - window // 2, 0)
        high = jnp.minimum(rows + window - window // 2, SEQ)
        mats.append(((cols >= low) & (cols < high)).astype(jnp.bfloat16))
    return mats


def pooling(pool_input):
    channels = pool_input.shape[1]
    group = channels // 4
    values = pool_input.reshape(-1, SEQ, channels)
    position = jnp.arange(SEQ)
    parts = []
    for index, (window, members) in enumerate(zip(WINDOWS, window_weights())):
        own = values[:, :, index * group:(index + 1) * group]
        sums = jnp.einsum("pq,sqc->spc", members, own, preferred_element_type=jnp.float32)
        before = window // 2
        counts = (
            jnp.minimum(position + window - before, SEQ) - jnp.maximum(position - before, 0)
        ).astype(jnp.float32)
        parts.append(sums / counts[None, :, None] - own.astype(jnp.float32))
    return jnp.concatenate(parts, axis=2).reshape(-1, channels).astype(jnp.bfloat16)


def body(
    nfs, ntp,
    stream, gain_first, gain_mixer, gain_second,
    gate_weight, gate_scale, up_weight, up_scale, down_weight, down_scale,
    pool_in_weight, pool_in_scale, pool_out_weight, pool_out_scale,
):
    half = jnp.bfloat16
    in_half, out_half = pool_in_weight.astype(half), pool_out_weight.astype(half)
    in_rows, in_cols = in_half.shape
    out_rows, out_cols = out_half.shape
    pool = jnp.concatenate([in_half, out_half.reshape(-1, in_cols)], axis=0)
    pool_all, gate_all, up_all, down_all, stream_all = gather_all(
        nfs, ntp, pool, gate_weight.astype(half), up_weight.astype(half), down_weight.astype(half), stream
    )
    in_whole = pool_all[:, :, :in_rows].transpose(1, 2, 0, 3).reshape(nfs * in_rows, ntp * in_cols)
    out_whole = (
        pool_all[:, :, in_rows:].reshape(ntp, nfs, out_rows, out_cols)
        .transpose(0, 2, 1, 3).reshape(ntp * out_rows, nfs * out_cols)
    )
    gate_whole = gate_all.reshape(-1, gate_all.shape[-1])
    up_whole = up_all.reshape(-1, up_all.shape[-1])
    down_whole = jnp.swapaxes(down_all, 0, 1).reshape(down_all.shape[1], -1)
    in_scale = lax.all_gather(pool_in_scale, "tp", tiled=True)
    out_scale = lax.all_gather(pool_out_scale, "tp", tiled=True)
    tp = lax.axis_index("tp")

    def feed_forward(rows):
        gate_sum = jnp.dot(rows, gate_whole, preferred_element_type=jnp.float32) * gate_scale
        up_sum = jnp.dot(rows, up_whole, preferred_element_type=jnp.float32) * up_scale
        hidden = (jax.nn.silu(gate_sum) * up_sum).astype(half)
        return jnp.dot(hidden, down_whole, preferred_element_type=jnp.float32).astype(half)

    first = rms(joined(stream_all).astype(jnp.float32), gain_first)
    after_first = joined(summed(ntp, True, 1, feed_forward(first), stream, down_scale))
    mixer_normed = rms(after_first.astype(jnp.float32), gain_mixer)
    pool_input = (
        jnp.dot(mixer_normed, in_whole, preferred_element_type=jnp.float32) * in_scale
    ).astype(half)
    mixed = jnp.dot(pooling(pool_input), out_whole, preferred_element_type=jnp.float32)
    after_mix = (after_first.astype(jnp.float32) + mixed * out_scale).astype(half)
    second = rms(after_mix.astype(jnp.float32), gain_second)
    own = lax.dynamic_slice_in_dim(after_mix, tp * stream.shape[1], stream.shape[1], axis=1)
    return summed(ntp, False, 2, feed_forward(second), own, down_scale)


def solution(mesh):
    placed = (
        P("fs", "tp"), P(), P(), P(),
        P("fs", "tp"), P("tp"), P("fs", "tp"), P("tp"), P("tp", "fs"), P("tp"),
        P("fs", "tp"), P("tp"), P("tp", "fs"), P("tp"),
    )
    return jax.shard_map(
        functools.partial(body, mesh.shape["fs"], mesh.shape["tp"]),
        mesh=mesh, in_specs=placed, out_specs=P("fs", "tp"), check_vma=False,
    )
```

time: 510 us -> 313 us (0.61)
  waiting for transfers between devices: 366 us -> 0 us
  Pallas kernels: 0 us -> 220 us
  blocking collectives: 69.9 us -> 10.9 us
  local copies, waits for them, and re-layouts: 1.86 us -> 40.8 us
  between operations: 13.8 us -> 0.38 us
  other arithmetic: 14.9 us -> 5.78 us
  matrix products: 39.5 us -> 34.2 us
    all_gather x6 -> x0, waiting for transfers between devices: 311 us -> none  [the longest x1 93.2 us: body(): lax.all_gather(down_half, 'fs', axis=1, tiled=True)]
    pallas_call x0 -> x3, Pallas kernels: none -> 220 us  [the longest x1 185 us: gather_all(): pl.pallas_call(functools.partial(gather_kernel, nfs, ntp), name='collect_...]
    all_gather x3 -> x2, blocking collectives: 69.9 us -> 10.9 us  [the longest x1 5.82 us: body(): out_scale = lax.all_gather(pool_out_scale, 'tp', tiled=True)]
    reduce_scatter x2 -> x0, waiting for transfers between devices: 54.4 us -> none  [residual_add(): lax.psum_scatter(partial_value.astype(jnp.bfloat16), 'tp', scatter_dimens...]
    unnamed x36 -> x47, local copies, waits for them, and re-layouts: 0.68 us -> 15.4 us
    transpose x0 -> x3, local copies, waits for them, and re-layouts: none -> 14.1 us  [the longest x1 8.27 us: body(): down_whole = jnp.swapaxes(down_all, 0, 1).reshape(down_all.shape[1], -1)]
    reshape x6 -> x3, local copies, waits for them, and re-layouts: 0.02 us -> 6.92 us  [the longest x2 6.89 us: body(): pool_all[:, :, in_rows:].reshape(ntp, nfs, out_rows, out_cols)]
    convert_element_type x12 -> x10, other arithmetic: 9.24 us -> 4.1 us  [the longest x1 1.55 us: body(): gate_weight.astype(half)]
  transfers between devices with their start and end apart: 9 -> 0, of which waited for: 7 -> 0; matrix products, arithmetic and copies ran while one was open for 4% -> 0% of each run, Pallas kernels for 0% -> 0%
where the time goes in v1:
time: 313 us
  Pallas kernels  220 us (70%)
  local copies, waits for them, and re-layouts  40.8 us (13%)
  matrix products  34.2 us (11%)
  blocking collectives  10.9 us (3%)
  other arithmetic  5.78 us (2%)
    pallas_call x1, Pallas kernels, gather_all(): pl.pallas_call(functools.partial(gather_kernel, nfs, ntp), name='collect_...  185 us
    pallas_call x2, Pallas kernels, summed(): pl.pallas_call(functools.partial(sum_kernel, ntp, gathers, pieces), name=...  35.5 us
    dot_general x2, matrix products, feed_forward(): jnp.dot(hidden, down_whole, preferred_element_type=jnp.float32).astype(half)  20.3 us
    unnamed x47, local copies, waits for them, and re-layouts  15.4 us
    dot_general x2, matrix products, feed_forward(): jnp.dot(rows, gate_whole, preferred_element_type=jnp.float32) * gate_scale  10.7 us
    transpose x1, local copies, waits for them, and re-layouts, body(): down_whole = jnp.swapaxes(down_all, 0, 1).reshape(down_all.shape[1], -1)  8.27 us
    reshape x2, local copies, waits for them, and re-layouts, body(): pool_all[:, :, in_rows:].reshape(ntp, nfs, out_rows, out_cols)  6.89 us

profile of v1, /device:TPU:0, one launch (start us, length us, event | category | flops | bytes accessed | tf_op | source)
XLA Modules:
  0.0 312.5 jit_solution(3825701406052599885)
XLA Ops:
  0.0 1.0 convert_element_type.123
  1.1 0.9 convert_element_type.122
  2.0 0.0 copy-start.11
  2.0 1.6 convert_element_type.124.gate
  3.6 0.0 copy-start.4
  3.6 0.1 convert_element_type.125.up
  3.7 0.1 copy-done.11
  3.8 0.1 convert_element_type.126.down
  3.9 0.8 copy-done.4
  4.6 184.9 %collect_weights.1 = (bf16[4,8,512,128]{3,2,1,0:T(8,128)(2,1)S(1)}, bf16[8,256,1408]{2,1,0:T(8,128)(2,1)S(1)}, bf16[8,256,1408]{2,1,0:T(8,128)(2,1)S(1)}, bf16[8...) custom-call(bf16[512,128]{1,0:T(8,128)(2,1)S(1)} %pad_maximum_fusion.pool, ...), custom_call_target="tpu_custom_call" | custom-call | tf_op jit(solution)/shard_map/collect_weights/pallas_call | solution.py:215
  189.5 2.5 copy-done
  192.0 2.5 copy-done.1
  194.5 2.0 copy-done.2
  196.6 2.5 copy-done.6
  199.0 8.3 %copy.23 = bf16[1408,8,256]{0,2,1:T(8,128)(2,1)} copy(bf16[1408,8,256]{2,0,1:T(8,128)(2,1)} %bitcast.88) | data formatting | bytes 11534336 | tf_op jit(solution)/shard_map/transpose | solution.py:410
  207.3 0.4 fusion
  207.7 0.4 fusion.14
  208.2 0.9 copy.22
  209.1 6.6 %convolution_multiply_fusion.3 = f32[384,1408]{1,0:T(8,128)} fusion(bf16[384,2048]{0,1:T(8,128)(2,1)S(1)} %bitcast.93, bf16[2048,1408]{1,0:T(8,128)(2,1)} %bitcast.84, f32[1408]{0:T(1024)S(1)} %copy-done.12), kind=kOutput, calls=%fused_computation.22 | convolution fusion | flops 2215133184 | bytes 9508352 | tf_op jit(solution)/shard_map/dot_general | solution.py:416
  215.7 10.3 %convolution_convert_fusion.1.partial = bf16[384,2048]{1,0:T(8,128)(2,1)S(1)} fusion(bf16[1408,2048]{0,1:T(8,128)(2,1)} %bitcast.97, bf16[384,2048]{0,1:T(8,128)(2,1)S(1)} %bitcast.94, bf16[2048,1408]{1,0:T(8,128)(2,1)} %bitcast.91, f32[384,1408]{1,0:T(8,128)} %convolution_multiply_fusion.3, f32[1408]{0:T(1024)} %param.21), kind=kOutput, calls=%fused_computation.24 | convolution fusion | flops 4433756160 | bytes 16848384 | tf_op jit(solution)/shard_map/dot_general | solution.py:419
  226.0 22.6 %sum_and_share.1 = bf16[4,384,512]{2,1,0:T(8,128)(2,1)S(1)} custom-call(bf16[384,2048]{1,0:T(8,128)(2,1)S(1)} %convolution_convert_fusion.1.partial, bf16[384,512]{1,0:T(8,128)(2,1)S(1)} %copy-done.4, f32[1,512]{1,0:T(1,128)S(1)} %bitcast.89), custom_call_target="tpu_custom_call" | custom-call | tf_op jit(solution)/shard_map/sum_and_share/pallas_call | solution.py:339
  248.6 0.4 convert_bitcast_fusion
  249.0 0.0 copy-start.16
  249.0 1.9 copy.28
  251.0 5.8 %all-gather.1 = f32[4,1,512]{2,1,0:T(1,128)} all-gather(f32[1,1,512]{2,1,0:T(1,128)S(1)} %bitcast.104), channel_id=1, replica_groups=mesh['fs'=8,'tp'=4] {'tp'}, dimensions={0}, use_global_device_ids=true | all-gather | bytes 10240 | tf_op jit(solution)/shard_map/all_gather | solution.py:412
  256.8 2.5 slice_bitcast_fusion
  259.2 4.1 %reshape.212 = bf16[4,8,128,256]{3,2,1,0:T(8,128)(2,1)} reshape(bf16[4,8,256,128]{3,2,1,0:T(8,128)(2,1)} %get-tuple-element.16) | data formatting | bytes 4194304 | tf_op jit(solution)/shard_map/reshape | solution.py:405
  263.4 2.8 copy.27
  266.1 0.0 copy-start.15
  266.2 2.0 copy.30
  268.2 0.4 fusion.6
  268.6 0.4 fusion.13
  269.0 1.6 copy.25
  270.7 3.3 %copy.26 = bf16[8,256,4,128]{1,0,3,2:T(8,128)(2,1)S(1)} copy(bf16[8,256,4,128]{3,1,0,2:T(8,128)(2,1)} %get-tuple-element.15) | data formatting | bytes 4194304 | tf_op jit(solution)/shard_map/transpose | solution.py:403
  274.0 0.7 copy.29
  274.7 5.1 %all-gather = f32[4,1,128]{2,1,0:T(1,128)S(1)} all-gather(f32[1,1,128]{2,1,0:T(1,128)S(1)} %bitcast.106), channel_id=1, replica_groups=mesh['fs'=8,'tp'=4] {'tp'}, dimensions={0}, use_global_device_ids=true | all-gather | bytes 2560 | tf_op jit(solution)/shard_map/all_gather | solution.py:411
  279.8 1.0 fusion.15
  280.9 0.2 fusion.27
  281.1 0.2 fusion.26
  281.4 0.2 fusion.25
  281.7 0.2 fusion.24
  281.9 0.9 copy-done.7
  282.9 1.2 fusion.3
  284.1 0.5 slice-done.1
  284.6 4.0 %convolution_multiply_fusion.1 = f32[384,1408]{1,0:T(8,128)} fusion(bf16[2048,1408]{1,0:T(8,128)(2,1)S(1)} %bitcast.87, f32[1408]{0:T(1024)S(1)} %copy-done.12, bf16[384,2048]{1,0:T(8,128)(2,1)S(1)} %get-tuple-element.18, f32[2048]{0:T(1024)S(1)} %copy-done.19, f32[384]{0:T(512)S(1)} %add_rsqrt_fusion), kind=kOutput, calls=%fused_computation.19 | convolution fusion | flops 2218278912 | bytes 9518080 | tf_op jit(solution)/shard_map/dot_general | solution.py:416
  288.7 10.1 %convolution_convert_fusion.partial = bf16[384,2048]{1,0:T(8,128)(2,1)S(1)} fusion(bf16[1408,2048]{0,1:T(8,128)(2,1)} %bitcast.98, bf16[2048,1408]{1,0:T(8,128)(2,1)} %bitcast.92, f32[384,1408]{1,0:T(8,128)} %convolution_multiply_fusion.1, f32[1408]{0:T(1024)S(1)} %copy-done.18, bf16[384,2048]{1,0:T(8,128)(2,1)S(1)} %get-tuple-element.18, ...), kind=kOutput, calls=%fused_computation.23 | convolution fusion | flops 4436901888 | bytes 16858112 | tf_op jit(solution)/shard_map/dot_general | solution.py:419
  298.8 13.0 %sum_last.1 = bf16[384,512]{1,0:T(8,128)(2,1)S(1)} custom-call(bf16[384,2048]{1,0:T(8,128)(2,1)S(1)} %convolution_convert_fusion.partial, bf16[384,512]{1,0:T(8,128)(2,1)S(1)} %constant_dynamic-slice_fusion.resid, f32[1,512]{1,0:T(1,128)S(1)} %bitcast.90), custom_call_target="tpu_custom_call" | custom-call | tf_op jit(solution)/shard_map/sum_last/pallas_call | solution.py:339
  311.8 0.7 copy.32
  (49 shorter events, 0.2 us)
Async XLA Ops:
  0.0 3.6 %copy-start.10 = (f32[256,1408]{1,0:T(8,128)S(1)}, f32[256,1408]{1,0:T(8,128)}, u32[]{:S(2)}) copy-start(f32[256,1408]{1,0:T(8,128)} %param.20) | copy-start | bytes 4325380
  2.0 1.8 copy-start.11
  3.6 1.1 copy-start.4
  189.5 2.5 copy-start
  192.0 2.5 copy-start.1
  194.5 2.0 copy-start.2
  196.6 2.5 copy-start.6
  199.0 8.3 %copy-start.14 = (f32[2048]{0:T(1024)S(1)}, f32[2048]{0:T(1024)}, u32[]{:S(2)}) copy-start(f32[2048]{0:T(1024)} %param.15) | copy-start | bytes 24580
  208.1 0.9 copy-start.12
  215.7 10.3 %copy-start.5 = (f32[512]{0:T(512)S(1)}, f32[512]{0:T(512)}, u32[]{:S(2)}) copy-start(f32[512]{0:T(512)} %param.23) | copy-start | bytes 6148
  249.0 2.0 copy-start.16
  249.0 7.8 %copy-start.3 = (bf16[4,8,512,128]{3,2,1,0:T(8,128)(2,1)S(1)}, bf16[4,8,512,128]{3,2,1,0:T(8,128)(2,1)}, u32[]{:S(2)}) copy-start(bf16[4,8,512,128]{3,2,1,0:T(8,128)(2,1)} %copy-done.2) | copy-start | bytes 12582916
  266.1 2.0 copy-start.15
  274.0 0.7 copy-start.17
  274.0 5.8 %copy-start.9 = (bf16[384,4,512]{0,2,1:T(8,128)(2,1)S(1)}, bf16[384,4,512]{0,2,1:T(8,128)(2,1)}, u32[]{:S(2)}) copy-start(bf16[384,4,512]{0,2,1:T(8,128)(2,1)} %copy.25) | copy-start | bytes 4718596
  279.8 2.1 copy-start.8
  280.8 2.0 copy-start.7
  280.8 2.0 copy-start.13
  280.9 3.2 %slice-start = ((s8[5767168]{0:T(1024)(128)(4,1)}), s8[4194304]{0:T(1024)(128)(4,1)S(1)}, s32[]{:S(2)}) async-start(s8[5767168]{0:T(1024)(128)(4,1)} %bitcast.85), calls=%async_computation | async-start | bytes 8388608
  282.9 1.7 slice-start.1
  282.9 1.7 copy-start.19
  284.6 4.1 %copy-start.18 = (f32[1408]{0:T(1024)S(1)}, f32[1408]{0:T(1024)}, u32[]{:S(2)}) copy-start(f32[1408]{0:T(1024)} %param.21) | copy-start | bytes 16900

commit v2 on v1

--- a/solution.py
+++ b/solution.py
@@ -21,8 +21,33 @@
     return ny, count // ny
 
 
-def gather_kernel(nfs, ntp, pool, gate, up, down, stream, pool_all, gate_all, up_all, down_all, stream_all,
-                  send_sem, recv_sem, local_sem, tsend, trecv, psend, precv):
+def grid_shape(row_blocks, col_blocks, block):
+    rows, cols = block
+    if cols % 128 == 0:
+        return (row_blocks * rows, col_blocks * cols)
+    return (row_blocks, col_blocks, rows, cols)
+
+
+def place(whole, block, row_block, col_block, part=(0, None)):
+    rows, cols = block
+    first, count = part[0], rows if part[1] is None else part[1]
+    if len(whole.shape) == 2:
+        return whole.at[
+            pl.ds(pl.multiple_of(row_block * rows + first, 16), count),
+            pl.ds(pl.multiple_of(col_block * cols, 128), cols),
+        ]
+    return whole.at[row_block, col_block, pl.ds(first, count)]
+
+
+def flat(whole):
+    if whole.ndim == 2:
+        return whole
+    return whole.transpose(0, 2, 1, 3).reshape(whole.shape[0] * whole.shape[2], -1)
+
+
+def gather_kernel(nfs, ntp, pool_in, pool_out, gate, up, down, stream, scales,
+                  in_all, out_all, gate_all, up_all, down_all, stream_all, scales_all,
+                  send_sem, recv_sem, local_sem, tsend, trecv, psend, precv, ssend, srecv):
     ny, nz = fs_grid(nfs)
     nx = ntp // 2
     fs, tp = lax.axis_index("fs"), lax.axis_index("tp")
@@ -42,26 +67,33 @@
     greet(z < nz - 1, fs + ny, tp)
     greet(y > 0, fs - 1, tp)
     greet(y < ny - 1, fs + 1, tp)
-    pl.semaphore_signal(barrier, inc=1, device_id={"fs": fs, "tp": partner}, device_id_type=MESH)
-    for k in range(1, nx):
+    for k in range(1, ntp):
         pl.semaphore_signal(
-            barrier, inc=1, device_id={"fs": fs, "tp": (x + k) % nx * 2 + core}, device_id_type=MESH
+            barrier, inc=1, device_id={"fs": fs, "tp": (tp + k) % ntp}, device_id_type=MESH
         )
-    peers = nx
+    peers = ntp - 1
     for cond in (z > 0, z < nz - 1, y > 0, y < ny - 1):
         peers = peers + jnp.where(cond, 1, 0)
     pl.semaphore_wait(barrier, peers)
 
-    pieces = [(lambda: pool, lambda f: pool_all.at[tp, f])]
-    for own, whole in ((gate, gate_all), (up, up_all), (down, down_all)):
+    pieces = [
+        (lambda: pool_in, lambda f: place(in_all, pool_in.shape, f, tp)),
+        (lambda: pool_out, lambda f: place(out_all, pool_out.shape, tp, f)),
+    ]
+    npool = len(pieces)
+    for own, whole, by_rows in ((gate, gate_all, True), (up, up_all, True), (down, down_all, False)):
         rows = own.shape[0]
         halves = 2 if alternate else 1
         for h in range(halves):
-            part = pl.ds(h * (rows // halves), rows // halves)
-            pieces.append((
-                functools.partial(lambda own, part: own.at[part], own, part),
-                functools.partial(lambda whole, part, f: whole.at[f, part], whole, part),
-            ))
+            part = (h * (rows // halves), rows // halves)
+
+            def own_part(own=own, part=part):
+                return own.at[pl.ds(*part)]
+
+            def whole_part(f, own=own, whole=whole, part=part, by_rows=by_rows):
+                return place(whole, own.shape, f if by_rows else 0, 0 if by_rows else f, part)
+
+            pieces.append((own_part, whole_part))
     started = []
 
     def remote(piece, f, direction, target, mine=False):
@@ -95,19 +127,40 @@
 
     yes = z >= 0
 
+    def stream_place(slot):
+        return place(stream_all, stream.shape, 0, slot)
+
     def stream_copy(src, slot, t_target, k):
         return pltpu.make_async_remote_copy(
-            src_ref=src, dst_ref=stream_all.at[slot], send_sem=tsend.at[k], recv_sem=trecv.at[slot],
+            src_ref=src, dst_ref=stream_place(slot), send_sem=tsend.at[k], recv_sem=trecv.at[slot],
             device_id={"fs": fs, "tp": t_target}, device_id_type=MESH)
 
-    def pool_copy(slot, t_target, k):
+    def slab(which, slot):
+        if which == 0:
+            if len(in_all.shape) == 2:
+                cols = pool_in.shape[1]
+                return in_all.at[:, pl.ds(pl.multiple_of(slot * cols, 128), cols)]
+            return in_all.at[:, slot]
+        if len(out_all.shape) == 2:
+            rows = pool_out.shape[0]
+            return out_all.at[pl.ds(pl.multiple_of(slot * rows, 16), rows)]
+        return out_all.at[slot]
+
+    def pool_copy(which, slot, t_target, k):
         return pltpu.make_async_remote_copy(
-            src_ref=pool_all.at[slot], dst_ref=pool_all.at[slot], send_sem=psend.at[k], recv_sem=precv.at[slot],
+            src_ref=slab(which, slot), dst_ref=slab(which, slot),
+            send_sem=psend.at[which, k], recv_sem=precv.at[which, slot],
+            device_id={"fs": fs, "tp": t_target}, device_id_type=MESH)
+
+    def scale_copy(k, slot, t_target):
+        return pltpu.make_async_remote_copy(
+            src_ref=scales, dst_ref=scales_all.at[slot], send_sem=ssend.at[k], recv_sem=srecv.at[slot],
             device_id={"fs": fs, "tp": t_target}, device_id_type=MESH)
 
     npieces = len(pieces)
     locals_ = [pltpu.make_async_copy(own(), whole(fs), local_sem.at[i]) for i, (own, whole) in enumerate(pieces)]
-    locals_.append(pltpu.make_async_copy(stream, stream_all.at[tp], local_sem.at[npieces]))
+    locals_.append(pltpu.make_async_copy(stream, stream_place(tp), local_sem.at[npieces]))
+    locals_.append(pltpu.make_async_copy(scales, scales_all.at[tp], local_sem.at[npieces + 1]))
     for piece in range(npieces):
         send(z > 0, piece, fs, 0, True)
         send(z < nz - 1, piece, fs, 1, True)
@@ -116,6 +169,7 @@
     for k in range(1, nx):
         stream_sends.append(stream_copy(stream, tp, (x + k) % nx * 2 + core, k - 1))
     stream_sends.append(stream_copy(stream, tp, partner, nx - 1))
+    stream_sends += [scale_copy(k - 1, tp, (tp + k) % ntp) for k in range(1, ntp)]
     for copy in stream_sends:
         copy.start()
     for copy in locals_:
@@ -157,20 +211,23 @@
                         if ny > 2:
                             send(row_ok & ok & ahead, piece, base + step, direction)
 
-    is_alt = [alternate and p > 0 and p % 2 == 0 for p in range(npieces)]
+    is_alt = [alternate and p >= npool and p % 2 == 1 for p in range(npieces)]
 
     for d in range(1, nz):
-        row_arrivals(0, d, False)
-    column_arrivals(0, False)
-    locals_[0].wait()
-    pool_sends = [pool_copy(tp, (x + k) % nx * 2 + core, k - 1) for k in range(1, nx)]
-    pool_sends.append(pool_copy(tp, partner, nx - 1))
+        for p in range(npool):
+            row_arrivals(p, d, False)
+    pool_sends = []
+    for p in range(npool):
+        column_arrivals(p, False)
+        locals_[p].wait()
+        pool_sends += [pool_copy(p, tp, (x + k) % nx * 2 + core, k - 1) for k in range(1, nx)]
+        pool_sends.append(pool_copy(p, tp, partner, nx - 1))
     for copy in pool_sends:
         copy.start()
     for k in range(1, nx):
         slot = (x + k) % nx * 2 + core
         stream_copy(stream, slot, partner, 0).wait_recv()
-        copy = stream_copy(stream_all.at[slot], slot, partner, nx - 1 + k)
+        copy = stream_copy(stream_place(slot), slot, partner, nx - 1 + k)
         copy.start()
         stream_sends.append(copy)
 
@@ -181,22 +238,26 @@
             send(z == 0, p, other, 1)
             send(z == nz - 1, p, other, 0)
     for d in range(1, nz):
-        for p in range(1, npieces):
+        for p in range(npool, npieces):
             row_arrivals(p, d, is_alt[p])
         if d == 1:
             for k in range(1, nx):
                 slot = (x + k) % nx * 2 + core
-                pool_copy(slot, partner, 0).wait_recv()
-                copy = pool_copy(slot, partner, nx - 1 + k)
-                copy.start()
-                pool_sends.append(copy)
-    for p in range(1, npieces):
+                for p in range(npool):
+                    pool_copy(p, slot, partner, 0).wait_recv()
+                    copy = pool_copy(p, slot, partner, nx - 1 + k)
+                    copy.start()
+                    pool_sends.append(copy)
+    for p in range(npool, npieces):
         column_arrivals(p, is_alt[p])
     for k in range(nx):
         slot = (x + k) % nx * 2 + (1 - core)
         stream_copy(stream, slot, partner, 0).wait_recv()
-        pool_copy(slot, partner, 0).wait_recv()
-    for copy in locals_[1:]:
+        for p in range(npool):
+            pool_copy(p, slot, partner, 0).wait_recv()
+    for k in range(1, ntp):
+        scale_copy(0, (tp + k) % ntp, partner).wait_recv()
+    for copy in locals_[npool:]:
         copy.wait()
     for copy in stream_sends + pool_sends:
         copy.wait_send()
@@ -206,35 +267,40 @@
             remote(piece, f, direction, target, mine).wait_send()
 
 
-def gather_all(nfs, ntp, pool, gate, up, down, stream):
+def gather_all(nfs, ntp, pool_in, pool_out, gate, up, down, stream, scales):
     ny, nz = fs_grid(nfs)
     nx = ntp // 2
-    npieces = 7 if (ny == 2 and nz > 1) else 4
-    dtype = jnp.bfloat16
+    npieces = 8 if (ny == 2 and nz > 1) else 5
     any_spec = pl.BlockSpec(memory_space=pl.ANY)
+    shapes = (
+        grid_shape(nfs, ntp, pool_in.shape),
+        grid_shape(ntp, nfs, pool_out.shape),
+        grid_shape(nfs, 1, gate.shape),
+        grid_shape(nfs, 1, up.shape),
+        grid_shape(1, nfs, down.shape),
+        grid_shape(1, ntp, stream.shape),
+    )
+    dma = pltpu.SemaphoreType.DMA
     return pl.pallas_call(
         functools.partial(gather_kernel, nfs, ntp),
         name="collect_weights",
-        out_shape=(
-            jax.ShapeDtypeStruct((ntp, nfs) + pool.shape, dtype),
-            jax.ShapeDtypeStruct((nfs,) + gate.shape, dtype),
-            jax.ShapeDtypeStruct((nfs,) + up.shape, dtype),
-            jax.ShapeDtypeStruct((nfs,) + down.shape, dtype),
-            jax.ShapeDtypeStruct((ntp,) + stream.shape, dtype),
-        ),
-        in_specs=[any_spec] * 5,
-        out_specs=[any_spec] * 5,
+        out_shape=tuple(jax.ShapeDtypeStruct(shape, jnp.bfloat16) for shape in shapes)
+        + (jax.ShapeDtypeStruct((ntp,) + scales.shape, jnp.float32),),
+        in_specs=[any_spec] * 7,
+        out_specs=[any_spec] * 7,
         scratch_shapes=[
-            pltpu.SemaphoreType.DMA((npieces, nfs, 4)),
-            pltpu.SemaphoreType.DMA((npieces, nfs)),
-            pltpu.SemaphoreType.DMA((npieces + 1,)),
-            pltpu.SemaphoreType.DMA((2 * nx,)),
-            pltpu.SemaphoreType.DMA((ntp,)),
-            pltpu.SemaphoreType.DMA((2 * nx,)),
-            pltpu.SemaphoreType.DMA((ntp,)),
+            dma((npieces, nfs, 4)),
+            dma((npieces, nfs)),
+            dma((npieces + 2,)),
+            dma((2 * nx,)),
+            dma((ntp,)),
+            dma((2, 2 * nx)),
+            dma((2, ntp)),
+            dma((ntp,)),
+            dma((ntp,)),
         ],
         compiler_params=pltpu.CompilerParams(collective_id=0, has_side_effects=True, vmem_limit_bytes=1 << 20),
-    )(pool, gate, up, down, stream)
+    )(pool_in, pool_out, gate, up, down, stream, scales)
 
 
 def sum_kernel(ntp, gathers, pieces, partial, resid, scale, out, pair, pair_sum, cross, *sems):
@@ -293,30 +359,30 @@
         if not gathers:
             out[part] = result
             continue
-        out[tp, part] = result
+        out[part, columns(tp)] = result
         gather_send, gather_recv = sems[4:]
         for k in range(1, nx):
-            copy = remote(out.at[tp, part], out.at[tp, part], gather_send.at[k - 1, i], gather_recv.at[tp, i],
+            copy = remote(out.at[part, columns(tp)], out.at[part, columns(tp)], gather_send.at[k - 1, i], gather_recv.at[tp, i],
                           (x + k) % nx * 2 + core)
             copy.start()
             sends.append(copy)
-        copy = remote(out.at[tp, part], out.at[tp, part], gather_send.at[nx - 1, i], gather_recv.at[tp, i], partner)
+        copy = remote(out.at[part, columns(tp)], out.at[part, columns(tp)], gather_send.at[nx - 1, i], gather_recv.at[tp, i], partner)
         copy.start()
         sends.append(copy)
     if gathers:
         for k in range(1, nx):
             slot = (x + k) % nx * 2 + core
             for i, part in enumerate(parts):
-                remote(out.at[slot, part], out.at[slot, part], gather_send.at[0, i], gather_recv.at[slot, i],
+                remote(out.at[part, columns(slot)], out.at[part, columns(slot)], gather_send.at[0, i], gather_recv.at[slot, i],
                        partner).wait_recv()
-                copy = remote(out.at[slot, part], out.at[slot, part], gather_send.at[nx - 1 + k, i],
+                copy = remote(out.at[part, columns(slot)], out.at[part, columns(slot)], gather_send.at[nx - 1 + k, i],
                               gather_recv.at[slot, i], partner)
                 copy.start()
                 sends.append(copy)
         for k in range(nx):
             slot = (x + k) % nx * 2 + (1 - core)
             for i, part in enumerate(parts):
-                remote(out.at[slot, part], out.at[slot, part], gather_send.at[0, i], gather_recv.at[slot, i],
+                remote(out.at[part, columns(slot)], out.at[part, columns(slot)], gather_send.at[0, i], gather_recv.at[slot, i],
                        partner).wait_recv()
     for copy in sends:
         copy.wait_send()
@@ -339,7 +405,7 @@
     return pl.pallas_call(
         functools.partial(sum_kernel, ntp, gathers, pieces),
         name="sum_and_share" if gathers else "sum_last",
-        out_shape=jax.ShapeDtypeStruct(((ntp,) if gathers else ()) + (rows, width), jnp.bfloat16),
+        out_shape=jax.ShapeDtypeStruct((rows, width * (ntp if gathers else 1)), jnp.bfloat16),
         in_specs=[vmem] * 3,
         out_specs=vmem,
         scratch_shapes=scratch,
@@ -347,10 +413,6 @@
             collective_id=identity, has_side_effects=True, vmem_limit_bytes=32 << 20
         ),
     )(partial, resid, scale.reshape(1, width))
-
-
-def joined(blocks):
-    return jnp.swapaxes(blocks, 0, 1).reshape(blocks.shape[1], -1)
 
 
 def rms(floats, norm_gain):
@@ -394,22 +456,16 @@
 ):
     half = jnp.bfloat16
     in_half, out_half = pool_in_weight.astype(half), pool_out_weight.astype(half)
-    in_rows, in_cols = in_half.shape
-    out_rows, out_cols = out_half.shape
-    pool = jnp.concatenate([in_half, out_half.reshape(-1, in_cols)], axis=0)
-    pool_all, gate_all, up_all, down_all, stream_all = gather_all(
-        nfs, ntp, pool, gate_weight.astype(half), up_weight.astype(half), down_weight.astype(half), stream
+    width, channels = stream.shape[1], in_half.shape[1]
+    scales = jnp.concatenate([pool_in_scale, pool_out_scale]).reshape(1, -1)
+    in_all, out_all, gate_all, up_all, down_all, stream_all, scales_all = gather_all(
+        nfs, ntp, in_half, out_half, gate_weight.astype(half), up_weight.astype(half), down_weight.astype(half),
+        stream, scales,
     )
-    in_whole = pool_all[:, :, :in_rows].transpose(1, 2, 0, 3).reshape(nfs * in_rows, ntp * in_cols)
-    out_whole = (
-        pool_all[:, :, in_rows:].reshape(ntp, nfs, out_rows, out_cols)
-        .transpose(0, 2, 1, 3).reshape(ntp * out_rows, nfs * out_cols)
-    )
-    gate_whole = gate_all.reshape(-1, gate_all.shape[-1])
-    up_whole = up_all.reshape(-1, up_all.shape[-1])
-    down_whole = jnp.swapaxes(down_all, 0, 1).reshape(down_all.shape[1], -1)
-    in_scale = lax.all_gather(pool_in_scale, "tp", tiled=True)
-    out_scale = lax.all_gather(pool_out_scale, "tp", tiled=True)
+    in_whole, out_whole = flat(in_all), flat(out_all)
+    gate_whole, up_whole, down_whole = flat(gate_all), flat(up_all), flat(down_all)
+    in_scale = scales_all[:, 0, :channels].reshape(-1)
+    out_scale = scales_all[:, 0, channels:].reshape(-1)
     tp = lax.axis_index("tp")
 
     def feed_forward(rows):
@@ -418,8 +474,8 @@
         hidden = (jax.nn.silu(gate_sum) * up_sum).astype(half)
         return jnp.dot(hidden, down_whole, preferred_element_type=jnp.float32).astype(half)
 
-    first = rms(joined(stream_all).astype(jnp.float32), gain_first)
-    after_first = joined(summed(ntp, True, 1, feed_forward(first), stream, down_scale))
+    first = rms(flat(stream_all).astype(jnp.float32), gain_first)
+    after_first = summed(ntp, True, 1, feed_forward(first), stream, down_scale)
     mixer_normed = rms(after_first.astype(jnp.float32), gain_mixer)
     pool_input = (
         jnp.dot(mixer_normed, in_whole, preferred_element_type=jnp.float32) * in_scale

time: 313 us -> 272 us (0.87)
  local copies, waits for them, and re-layouts: 40.8 us -> 12.6 us
  blocking collectives: 10.9 us -> 0 us
  other arithmetic: 5.78 us -> 2.63 us
    transpose x3 -> x0, local copies, waits for them, and re-layouts: 14.1 us -> none  [the longest x1 8.27 us: body(): down_whole = jnp.swapaxes(down_all, 0, 1).reshape(down_all.shape[1], -1)]
    all_gather x2 -> x0, blocking collectives: 10.9 us -> none  [the longest x1 5.82 us: body(): out_scale = lax.all_gather(pool_out_scale, 'tp', tiled=True)]
    reshape x3 -> x1, local copies, waits for them, and re-layouts: 6.92 us -> 0.01 us  [body(): scales = jnp.concatenate([pool_in_scale, pool_out_scale]).reshape(1, -1)]
    unnamed x47 -> x50, local copies, waits for them, and re-layouts: 15.4 us -> 11.4 us
where the time goes in v2:
time: 272 us
  Pallas kernels  219 us (81%)
  matrix products  36.5 us (13%)
  local copies, waits for them, and re-layouts  12.6 us (5%)
    pallas_call x1, Pallas kernels, gather_all(): pl.pallas_call(functools.partial(gather_kernel, nfs, ntp), name='collect_...  185 us
    pallas_call x2, Pallas kernels, summed(): pl.pallas_call(functools.partial(sum_kernel, ntp, gathers, pieces), name=...  34.7 us
    dot_general x2, matrix products, feed_forward(): jnp.dot(hidden, down_whole, preferred_element_type=jnp.float32).astype(half)  20.6 us
    unnamed x50, local copies, waits for them, and re-layouts  11.4 us
    dot_general x2, matrix products, feed_forward(): jnp.dot(rows, gate_whole, preferred_element_type=jnp.float32) * gate_scale  10.9 us

profile of v2, /device:TPU:0, one launch (start us, length us, event | category | flops | bytes accessed | tf_op | source)
XLA Modules:
  0.0 271.6 jit_solution(12734682890409593270)
XLA Ops:
  0.0 1.6 convert_element_type.102.gate
  1.6 0.2 copy-done.8
  1.8 0.0 copy-start
  1.8 0.1 convert_element_type.103.up
  1.9 0.3 copy-done.9
  2.2 0.1 convert_element_type.104.down
  2.3 0.5 copy-done.10
  2.8 0.0 copy-done.11
  2.9 0.0 copy-done.13
  2.9 0.0 copy-done.15
  2.9 0.0 copy-start.16
  2.9 0.0 copy-start.18
  2.9 0.1 copy-done
  3.0 184.7 %collect_weights.1 = (bf16[2048,512]{1,0:T(8,128)(2,1)S(1)}, bf16[512,2048]{1,0:T(8,128)(2,1)S(1)}, bf16[2048,1408]{1,0:T(8,128)(2,1)S(1)}, bf16[2048,1408]{1,0:...) custom-call(bf16[256,128]{1,0:T(8,128)(2,1)S(1)} %convert_element_type.10, ...), custom_call_target="tpu_custom_call" | custom-call | tf_op jit(solution)/shard_map/collect_weights/pallas_call | solution.py:284
  187.7 0.0 copy-start.2
  187.8 2.5 copy-done.2
  190.3 2.5 copy-done.3
  192.8 1.3 copy-done.5
  194.1 1.4 copy-done.6
  195.5 0.4 fusion
  195.9 0.0 copy-done.16
  195.9 0.0 copy-done.18
  195.9 4.1 %convolution_multiply_fusion.3 = f32[384,1408]{1,0:T(8,128)} fusion(bf16[2048,1408]{1,0:T(8,128)(2,1)S(1)} %get-tuple-element.13, f32[1408]{0:T(1024)S(1)} %copy-done.18, bf16[384,2048]{1,0:T(8,128)(2,1)S(1)} %get-tuple-element.12, f32[2048]{0:T(1024)S(1)} %copy-done.16, f32[384]{0:T(512)S(1)} %add_rsqrt_fusion.2), kind=kOutput, calls=%fused_computation.22 | convolution fusion | flops 2218278912 | bytes 9518080 | tf_op jit(solution)/shard_map/dot_general | solution.py:472
  200.0 0.0 copy-done.4
  200.0 10.1 %convolution_convert_fusion.1.partial = bf16[384,2048]{1,0:T(8,128)(2,1)S(1)} fusion(bf16[1408,2048]{1,0:T(8,128)(2,1)} %copy-done.3, bf16[2048,1408]{1,0:T(8,128)(2,1)} %copy-done.2, f32[384,1408]{1,0:T(8,128)} %convolution_multiply_fusion.3, f32[1408]{0:T(1024)} %param.21, bf16[384,2048]{1,0:T(8,128)(2,1)S(1)} %get-tuple-element.12, f32[2048]{0:T(1024)} %param.15, ...), kind=kOutput, calls=%fused_computation.24 | convolution fusion | flops 4436901888 | bytes 16858112 | tf_op jit(solution)/shard_map/dot_general | solution.py:475
  210.1 0.0 copy-start.17
  210.1 21.7 %sum_and_share.1 = bf16[384,2048]{1,0:T(8,128)(2,1)S(1)} custom-call(bf16[384,2048]{1,0:T(8,128)(2,1)S(1)} %convolution_convert_fusion.1.partial, bf16[384,512]{1,0:T(8,128)(2,1)S(1)} %copy-done, f32[1,512]{1,0:T(1,128)S(1)} %bitcast.50), custom_call_target="tpu_custom_call" | custom-call | tf_op jit(solution)/shard_map/sum_and_share/pallas_call | solution.py:405
  231.9 0.4 fusion.6
  232.3 1.0 fusion.21
  233.3 0.1 fusion.68
  233.4 0.1 copy.24
  233.6 0.3 fusion.32
  233.8 0.1 copy.25
  234.0 0.3 fusion.33
  234.3 0.1 copy.26
  234.4 0.3 fusion.34
  234.7 0.1 copy.27
  234.8 0.3 fusion.35
  235.2 0.2 copy.23
  235.3 0.0 copy-start.19
  235.4 0.0 copy-start.21
  235.4 2.8 %fusion.3 = (f32[384]{0:T(512)S(1)}, bf16[384,2048]{1,0:T(8,128)(2,1)S(1)}) fusion(f32[2048]{0:T(1024)S(1)} %bitcast.58, bf16[384,512]{1,0:T(8,128)(2,1)S(1)} %bitcast.57, bf16[512,2048]{1,0:T(8,128)(2,1)} %copy-done.5, bf16[384,2048]{1,0:T(8,128)(2,1)S(1)} %sum_and_share.1), kind=kOutput, calls=%fused_computation.10 | convolution fusion | flops 810811008 | bytes 5645824 | tf_op jit(solution)/shard_map/dot_general | solution.py:483
  238.2 1.1 copy-done.12
  239.4 6.9 %convolution_multiply_fusion.1 = f32[384,1408]{1,0:T(8,128)} fusion(bf16[2048,1408]{1,0:T(8,128)(2,1)} %copy-done.4, f32[1408]{0:T(1024)S(1)} %copy-done.19, bf16[384,2048]{1,0:T(8,128)(2,1)S(1)} %get-tuple-element.24, f32[2048]{0:T(1024)S(1)} %copy-done.21, f32[384]{0:T(512)S(1)} %add_rsqrt_fusion), kind=kOutput, calls=%fused_computation.19 | convolution fusion | flops 2218278912 | bytes 9518080 | tf_op jit(solution)/shard_map/dot_general | solution.py:472
  246.3 10.5 %convolution_convert_fusion.partial = bf16[384,2048]{1,0:T(8,128)(2,1)S(1)} fusion(bf16[1408,2048]{1,0:T(8,128)(2,1)} %copy-done.3, bf16[2048,1408]{1,0:T(8,128)(2,1)} %copy-done.2, f32[384,1408]{1,0:T(8,128)} %convolution_multiply_fusion.1, f32[1408]{0:T(1024)S(1)} %copy-done.20, bf16[384,2048]{1,0:T(8,128)(2,1)} %copy-done.12, f32[2048]{0:T(1024)S(1)} %copy-done.21, ...), kind=kOutput, calls=%fused_computation.23 | convolution fusion | flops 4436901888 | bytes 16858112 | tf_op jit(solution)/shard_map/dot_general | solution.py:475
  256.8 1.0 constant_dynamic-slice_fusion.resid
  257.8 13.0 %sum_last.1 = bf16[384,512]{1,0:T(8,128)(2,1)S(1)} custom-call(bf16[384,2048]{1,0:T(8,128)(2,1)S(1)} %convolution_convert_fusion.partial, bf16[384,512]{1,0:T(8,128)(2,1)S(1)} %constant_dynamic-slice_fusion.resid, f32[1,512]{1,0:T(1,128)S(1)} %bitcast.51), custom_call_target="tpu_custom_call" | custom-call | tf_op jit(solution)/shard_map/sum_last/pallas_call | solution.py:405
  270.8 0.7 copy.29
  (40 shorter events, 0.2 us)
Async XLA Ops:
  0.0 1.8 copy-start.8
  0.0 2.2 copy-start.9
  1.8 1.0 copy-start.10
  1.8 1.0 copy-start.11
  1.8 1.1 copy-start.13
  1.8 1.1 copy-start.15
  1.8 1.2 copy-start
  2.9 193.0 %copy-start.16 = (f32[2048]{0:T(1024)S(1)}, f32[2048]{0:T(1024)}, u32[]{:S(2)}) copy-start(f32[2048]{0:T(1024)} %param.15) | copy-start | bytes 24580
  2.9 193.0 %copy-start.18 = (f32[1408]{0:T(1024)S(1)}, f32[1408]{0:T(1024)}, u32[]{:S(2)}) copy-start(f32[1408]{0:T(1024)} %param.19) | copy-start | bytes 16900
  187.7 2.5 copy-start.2
  190.3 2.5 copy-start.3
  192.8 1.4 copy-start.5
  194.1 1.4 copy-start.6
  195.5 4.5 %copy-start.4 = (bf16[2048,1408]{1,0:T(8,128)(2,1)}, bf16[2048,1408]{1,0:T(8,128)(2,1)S(1)}, u32[]{:S(2)}) copy-start(bf16[2048,1408]{1,0:T(8,128)(2,1)S(1)} %get-tuple-element.13) | copy-start | bytes 17301508
  195.9 4.1 %copy-start.14 = (f32[384]{0:T(512)}, f32[384]{0:T(512)S(1)}, u32[]{:S(2)}) copy-start(f32[384]{0:T(512)S(1)} %add_rsqrt_fusion.2) | copy-start | bytes 4612
  200.0 10.1 %copy-start.1 = (f32[512]{0:T(512)S(1)}, f32[512]{0:T(512)}, u32[]{:S(2)}) copy-start(f32[512]{0:T(512)} %param.23) | copy-start | bytes 6148
  210.1 22.2 %copy-start.7 = (bf16[2048,512]{1,0:T(8,128)(2,1)S(1)}, bf16[2048,512]{1,0:T(8,128)(2,1)}, u32[]{:S(2)}) copy-start(bf16[2048,512]{1,0:T(8,128)(2,1)} %copy-done.6) | copy-start | bytes 6291460
  210.1 22.2 %copy-start.17 = (f32[2048]{0:T(1024)S(1)}, f32[2048]{0:T(1024)}, u32[]{:S(2)}) copy-start(f32[2048]{0:T(1024)} %param.16) | copy-start | bytes 24580
  235.3 4.0 %copy-start.19 = (f32[1408]{0:T(1024)S(1)}, f32[1408]{0:T(1024)}, u32[]{:S(2)}) copy-start(f32[1408]{0:T(1024)} %param.19) | copy-start | bytes 16900
  235.4 4.0 %copy-start.21 = (f32[2048]{0:T(1024)S(1)}, f32[2048]{0:T(1024)}, u32[]{:S(2)}) copy-start(f32[2048]{0:T(1024)} %param.17) | copy-start | bytes 24580
  238.2 1.2 copy-start.12
  239.4 6.9 %copy-start.20 = (f32[1408]{0:T(1024)S(1)}, f32[1408]{0:T(1024)}, u32[]{:S(2)}) copy-start(f32[1408]{0:T(1024)} %param.21) | copy-start | bytes 16900
